TPU v7x, 32 devices: a whole 2x2x4 slice. The times are simulated.
32 devices in a mesh: sp: 4 (over z), tp: 8 (over y, x, core).
Axes of the slice: x: 2, y: 2, z: 4, core: 2. Of those that a mesh axis runs over, the one named last changes fastest.
Arguments:
- context_activations: bfloat16 [2, 1024, 4096], P(None, 'sp', 'tp'), may hold values from -6 to 6
- first_generated_activation: bfloat16 [2, 4096], replicated, may hold values from -6 to 6
- address_projection: bfloat16 [4096, 1024], P(None, 'tp'), may hold values from -0.09375 to 0.09375
- payload_projection: bfloat16 [4096, 1024], P(None, 'tp'), may hold values from -0.09375 to 0.09375
- lookup_projection: bfloat16 [4096, 1024], P(None, 'tp'), may hold values from -0.09375 to 0.09375
- exit_gating_projection: bfloat16 [4096, 1024], P(None, 'tp'), may hold values from -0.09375 to 0.09375
- writing_intensity_projection: bfloat16 [4096, 8], replicated, may hold values from -0.09375 to 0.09375
- fading_projection: bfloat16 [4096, 8], replicated, may hold values from -0.09375 to 0.09375
- channel_fading_speed: float32 [8], replicated, may hold values from 0 to 1, as said below
- extra_fading_log: float32 [2, 1024, 8], P(None, 'sp', 'tp'), may hold values from -1 to 0, as said below
- readout_normalizer_gain: float32 [128], replicated, may hold values from 0.1 to 1.9
- exit_projection: bfloat16 [1024, 4096], P('tp'), may hold values from -0.1875 to 0.1875
Outputs:
- state_cache: bfloat16 [2, 4, 8, 128, 128], P(None, 'sp', 'tp')
- step_out: bfloat16 [2, 4096], P(None, 'tp')
Inputs may be any that keep to these rules, and one draw needn't show every extreme that they name: `channel_fading_speed`: positive rates, one a head. `extra_fading_log`: zero at all but a few positions of each prompt and head, negative there.
All inputs are finite; a program needn't handle non-finite values.
Results may differ from a plain program's by a relative error of at most 0.012.
Values may be sent and summed in bfloat16 or wider, within the bound.
A program may use at most 64 MiB of HBM per device.

v0:
```python
import jax
import jax.numpy as jnp
from jax import lax
from jax.sharding import PartitionSpec as P

BLOCK = 64


norm_eps = 1e-06
highest = lax.Precision.HIGHEST


def carried_in(value, axis, combine, identity):
    devices, position = (lax.axis_size(axis), lax.axis_index(axis))
    everything = jax.tree.map(
        lambda part, kind: lax.all_gather(part.astype(kind), axis),
        value,
        (jnp.bfloat16, jnp.bfloat16),
    )
    start = jax.tree.map(
        lambda part, zero: jnp.broadcast_to(jnp.asarray(zero, part.dtype), part.shape),
        value,
        identity,
    )

    def lap(k, before):
        reached = k < position
        new = combine(
            before, jax.tree.map(lambda part, own: part[k].astype(own.dtype), everything, value)
        )
        return jax.tree.map(lambda a, b: jnp.where(reached, a, b), new, before)

    return lax.fori_loop(0, devices, lap, start)


def carried_in_2(value, axis, combine, identity):
    devices, position = (lax.axis_size(axis), lax.axis_index(axis))
    everything = lax.all_gather(value, axis)
    start = jnp.broadcast_to(jnp.asarray(identity, value.dtype), value.shape)

    def lap(k, before):
        at = devices - 1 - k
        reached = at > position
        new = combine(before, everything[at])
        return jnp.where(reached, new, before)

    return lax.fori_loop(0, devices, lap, start)


def unit_rows(values_in):
    return values_in * lax.rsqrt(jnp.sum(values_in * values_in, axis=-1, keepdims=True) + norm_eps)


def compose(left, right):
    return jnp.einsum("...ij,...jk->...ik", left, right, precision=highest)


def segment_map(keys_in, values_in, beta_gate, fading_exponent):
    blocks = keys_in.shape[0] // BLOCK
    key_blocks = keys_in.reshape(blocks, BLOCK, -1)
    value_blocks = values_in.reshape(blocks, BLOCK, -1)
    beta_blocks = beta_gate.reshape(blocks, BLOCK)
    cumul = jnp.cumsum(fading_exponent.reshape(blocks, BLOCK), axis=-1)
    causal = jnp.tril(jnp.ones((BLOCK, BLOCK), bool))
    strict = jnp.tril(jnp.ones((BLOCK, BLOCK), bool), -1)
    gaps_log = cumul[:, :, None] - cumul[:, None, :]
    within = jnp.where(causal, jnp.exp(jnp.where(causal, gaps_log, 0.0)), 0.0)
    keys_beta = key_blocks * beta_blocks[..., None]
    strict_part = jnp.where(
        strict, jnp.einsum("nid,njd->nij", keys_beta, key_blocks, precision=highest) * within, 0.0
    )
    targets = jnp.concatenate(
        [value_blocks * beta_blocks[..., None], keys_beta * jnp.exp(cumul)[..., None]], axis=-1
    )
    system = jnp.eye(BLOCK, dtype=jnp.float32) + strict_part
    solved = lax.linalg.triangular_solve(system, targets, left_side=True, lower=True)
    width_v = value_blocks.shape[-1]
    width_k = key_blocks.shape[-1]
    pseudo_values = solved[..., :width_v]
    decayed_keys = solved[..., width_v:]
    carried_values = jnp.concatenate(
        [jnp.zeros((blocks, BLOCK, width_k), jnp.float32), pseudo_values], axis=-1
    )
    trailing = key_blocks * jnp.exp(cumul[:, -1:] - cumul)[..., None]
    block_decay = jnp.exp(cumul[:, -1])

    def advance(memory, inputs):
        pseudo, decayed, trail_keys, shrink = inputs
        fresh_values = pseudo - jnp.dot(decayed, memory, precision=highest)
        memory = memory * shrink + jnp.dot(trail_keys.T, fresh_values, precision=highest)
        return (memory, None)

    start_map = jnp.concatenate(
        [jnp.eye(width_k, dtype=jnp.float32), jnp.zeros((width_k, width_v), jnp.float32)], axis=1
    )
    memory, _ = lax.scan(advance, start_map, (carried_values, decayed_keys, trailing, block_decay))
    return memory


def combine_maps(earlier, later):
    return (compose(later[0], earlier[0]), compose(later[0], earlier[1]) + later[1])


def body(
    context_activations,
    first_generated_activation,
    address_projection,
    payload_projection,
    lookup_projection,
    exit_gating_projection,
    writing_intensity_projection,
    fading_projection,
    channel_fading_speed,
    extra_fading_log,
    readout_normalizer_gain,
    exit_projection,
):
    head_size = readout_normalizer_gain.shape[0]
    current_heads = address_projection.shape[1] // head_size
    first_head = lax.axis_index("tp") * current_heads
    beta_cols = lax.dynamic_slice_in_dim(writing_intensity_projection, first_head, current_heads, 1)
    decay_cols = lax.dynamic_slice_in_dim(fading_projection, first_head, current_heads, 1)
    logit_weight = jnp.concatenate([beta_cols, decay_cols], axis=1)
    fading_speeds = lax.dynamic_slice_in_dim(channel_fading_speed, first_head, current_heads, 0)
    seq_count, length = (context_activations.shape[0], context_activations.shape[1])
    portion = lax.all_gather(context_activations, "tp", axis=2, tiled=True)
    key_sum = jnp.einsum(
        "abf,fc->abc", portion, address_projection, preferred_element_type=jnp.float32
    )
    value_sum = jnp.einsum(
        "abf,fc->abc", portion, payload_projection, preferred_element_type=jnp.float32
    )
    logit_sum = jnp.einsum("abf,fc->abc", portion, logit_weight, preferred_element_type=jnp.float32)
    shaped = (seq_count, length, current_heads, head_size)
    keys_here = unit_rows(jax.nn.silu(key_sum).reshape(shaped)).astype(jnp.bfloat16)
    values_here = jax.nn.silu(value_sum).reshape(shaped).astype(jnp.bfloat16)
    current_scores = logit_sum.astype(jnp.bfloat16)
    beta_gate = jax.nn.sigmoid(current_scores[..., :current_heads].astype(jnp.float32))
    fading_exponent = extra_fading_log - fading_speeds * jax.nn.softplus(
        current_scores[..., current_heads:].astype(jnp.float32)
    )
    maps = jax.vmap(jax.vmap(segment_map, in_axes=(1, 1, 1, 1)))(
        keys_here.astype(jnp.float32), values_here.astype(jnp.float32), beta_gate, fading_exponent
    )
    own_moves = maps[..., :head_size]
    own_offset = maps[..., head_size:]
    heads_shape = (seq_count, current_heads, head_size)
    new_keys = unit_rows(
        jax.nn.silu(
            jnp.dot(
                first_generated_activation, address_projection, preferred_element_type=jnp.float32
            )
        ).reshape(heads_shape)
    )
    new_values = jax.nn.silu(
        jnp.dot(first_generated_activation, payload_projection, preferred_element_type=jnp.float32)
    ).reshape(heads_shape)
    new_queries = unit_rows(
        jax.nn.silu(
            jnp.dot(
                first_generated_activation, lookup_projection, preferred_element_type=jnp.float32
            )
        ).reshape(heads_shape)
    )
    out_gate = jax.nn.silu(
        jnp.dot(
            first_generated_activation, exit_gating_projection, preferred_element_type=jnp.float32
        )
    ).reshape(heads_shape)
    new_logits = jnp.dot(
        first_generated_activation, logit_weight, preferred_element_type=jnp.float32
    )
    new_beta = jax.nn.sigmoid(new_logits[:, :current_heads])
    new_decay = jnp.exp(-fading_speeds * jax.nn.softplus(new_logits[:, current_heads:]))
    intersection_kq = jnp.sum(new_keys * new_queries, axis=-1, keepdims=True)
    carried_query = new_decay[..., None] * (
        new_queries - new_beta[..., None] * new_keys * intersection_kq
    )
    own_write = new_beta[..., None] * new_values * intersection_kq
    identity = jnp.broadcast_to(jnp.eye(head_size, dtype=jnp.float32), own_moves.shape)
    prefix_moves, prefix_offset = carried_in(
        (own_moves, own_offset), "sp", combine_maps, (identity, jnp.zeros_like(own_offset))
    )
    states_here = compose(own_moves, prefix_offset) + own_offset

    def chain_later(earlier, later):
        return compose(earlier, later)

    later_moves = carried_in_2(own_moves, "sp", chain_later, identity)
    lifted = jnp.einsum("shjk,shj->shk", later_moves, carried_query, precision=highest)
    term = jnp.einsum("shk,shkv->shv", lifted, own_offset, precision=highest)
    read = lax.psum(term, "sp") + own_write
    state_cache = states_here.astype(jnp.bfloat16)[:, None]
    normed = (
        read
        * lax.rsqrt(jnp.mean(read * read, axis=-1, keepdims=True) + norm_eps)
        * readout_normalizer_gain
        * out_gate
    )
    normed = normed.astype(jnp.bfloat16).reshape(seq_count, current_heads * head_size)
    partial_out = jnp.dot(normed, exit_projection, preferred_element_type=jnp.float32)
    step_out = lax.psum_scatter(partial_out, "tp", scatter_dimension=1, tiled=True).astype(
        jnp.bfloat16
    )
    return (state_cache, step_out)


def solution(mesh):
    placed = (
        P(None, "sp", "tp"),
        P(),
        P(None, "tp"),
        P(None, "tp"),
        P(None, "tp"),
        P(None, "tp"),
        P(),
        P(),
        P(),
        P(None, "sp", "tp"),
        P(),
        P("tp", None),
    )
    return jax.shard_map(
        body,
        mesh=mesh,
        in_specs=placed,
        out_specs=(P(None, "sp", "tp", None, None), P(None, "tp")),
        check_vma=False,
    )
```

profile of v0, /device:TPU:0, one launch (start us, length us, event | category | flops | bytes accessed | tf_op | source)
XLA Modules:
  0.0 188.7 jit_solution(4630512967896987474)
XLA Ops:
  7.2 0.7 all-gather.5.cloned.1.call-update
  8.1 1.3 dynamic_slice.48
  10.2 1.6 multiply_reduce_fusion.4
  11.8 1.1 multiply_reduce_fusion.3
  13.1 0.9 constant_dynamic-slice_fusion.1
  14.0 0.9 convolution_bitcast_fusion.6
  15.1 34.9 %all-gather.5.cloned.1.call-done = bf16[2,256,4096]{2,1,0:T(8,128)(2,1)} async-done(((bf16[2,256,512]{2,1,0:T(8,128)(2,1)}), bf16[2,256,4096]{2,1,0:T(8,128)(2,1)}) %all-gather.5.cloned.1.call-update) | async-done | bytes 4194320 | tf_op jit(solution)/shard_map/all_gather | solution.py:126
  50.0 3.4 %fusion.31 = bf16[2,256,2]{1,2,0:T(2,128)(2,1)S(1)} fusion(bf16[2,256,4096]{2,1,0:T(8,128)(2,1)} %all-gather.5.cloned.1.call-done, bf16[4096,1]{0,1:T(2,128)(2,1)S(1)} %get-tuple-element.365, bf16[4096,1]{0,1:T(2,128)(2,1)S(1)} %get-tuple-element.366), kind=kOutput, calls=%fused_computation.41 | convolution fusion | flops 8422400 | bytes 4212736 | tf_op jit(solution)/shard_map/abf,fc->abc/dot_general | solution.py:133
  53.3 0.7 fusion.63
  55.0 3.6 %multiply_reduce_fusion = (f32[2,256]{1,0:T(2,128)S(1)}, f32[2,256,128]{2,1,0:T(8,128)S(1)}) fusion(bf16[2,256,4096]{2,1,0:T(8,128)(2,1)} %all-gather.5.cloned.1.call-done, bf16[4096,128]{1,0:T(8,128)(2,1)S(1)} %copy-done), kind=kOutput, calls=%fused_computation.60 | convolution fusion | flops 537263616 | bytes 5507072 | tf_op jit(solution)/shard_map/abf,fc->abc/dot_general | solution.py:127
  59.1 39.3 %custom-call.3 = f32[2,1,4,1,64,64]{4,5,3,2,1,0:T(8,128)S(1)} custom-call(f32[2,1,4,1,64,64]{5,4,3,2,1,0:T(8,128)S(1)} %fusion.27), custom_call_target="InvertDiagBlocksLowerTriangular" | custom-call | tf_op jit(solution)/shard_map/vmap(vmap())/triangular_solve | solution.py:76
  98.5 3.5 %multiply_convert_fusion = bf16[2,256,128]{2,1,0:T(8,128)(2,1)S(1)} fusion(bf16[2,256,4096]{2,1,0:T(8,128)(2,1)} %all-gather.5.cloned.1.call-done, bf16[4096,128]{1,0:T(8,128)(2,1)S(1)} %copy-done.5), kind=kOutput, calls=%fused_computation.56 | convolution fusion | flops 537198592 | bytes 5373952 | tf_op jit(solution)/shard_map/abf,fc->abc/dot_general | solution.py:130
  103.1 3.0 %while.39 = (s32[]{:T(128)}, f32[2,1,128,256]{3,2,0,1:T(8,128)S(1)}, f32[4,2,1]{1,2,0:T(1,128)S(1)}, f32[4,2,1,64,128]{4,3,0,1,2:T(8,128)S(1)}, f32[4,2,1,64,256...) while((s32[]{:T(128)}, f32[2,1,128,256]{3,2,0,1:T(8,128)S(1)}, ...), condition=%wide.region_3.4_spmd, body=%wide.region_2.3_spmd.sunk | while | flops 100827136 | bytes 1312357 | solution.py:96
  106.2 16.2 %all-gather.2 = f32[8,1,128,128]{3,2,1,0:T(8,128)S(1)} all-gather(f32[2,1,128,128]{3,2,1,0:T(8,128)S(1)} %slice_bitcast_fusion.1), channel_id=4, replica_groups=mesh['sp'=4,'tp'=8] {'sp'}, dimensions={0}, use_global_device_ids=true | all-gather | bytes 655360 | tf_op jit(solution)/shard_map/all_gather | solution.py:38
  122.4 1.8 while.40
  124.7 12.1 %psum.7 = f32[2,1,128]{2,0,1:T(2,128)S(1)} all-reduce(f32[2,1,128]{2,0,1:T(2,128)S(1)} %bitcast.222), channel_id=1, replica_groups=mesh['sp'=4,'tp'=8] {'sp'}, use_global_device_ids=true, to_apply=%region_11.12 | all-reduce | flops 256 | bytes 2048 | tf_op jit(solution)/shard_map/psum | solution.py:192
  136.8 1.6 multiply_reduce_fusion.1
  138.5 3.3 %convolution_bitcast_fusion.2 = f32[4096,2]{1,0:T(8,128)} fusion(bf16[128,4096]{1,0:T(8,128)(2,1)S(1)} %copy-done.1, f32[2,1,128]{2,0,1:T(2,128)S(1)} %get-tuple-element.345, f32[128]{0:T(128)S(1)} %copy-done.4, f32[2]{0:T(128)S(1)} %add_rsqrt_fusion.1, bf16[2,4096]{1,0:T(2,128)(2,1)S(1)} %copy-done.2, bf16[4096,128]{1,0:T(8,128)(2,1)} %param.23), kind=kOutput, calls=%fused_computation.29 | convolution fusion | flops 4196352 | bytes 2147848
  141.8 14.4 %all-gather = bf16[8,1,128,128]{3,2,1,0:T(8,128)(2,1)S(1)} all-gather(bf16[2,1,128,128]{3,2,1,0:T(8,128)(2,1)S(1)} %get-tuple-element.355), channel_id=2, replica_groups=mesh['sp'=4,'tp'=8] {'sp'}, dimensions={0}, use_global_device_ids=true | all-gather | bytes 327680 | tf_op jit(solution)/shard_map/all_gather | solution.py:16
  156.2 13.8 %all-gather.1 = bf16[8,1,128,128]{3,2,1,0:T(8,128)(2,1)S(1)} all-gather(bf16[2,1,128,128]{3,2,1,0:T(8,128)(2,1)S(1)} %get-tuple-element.354), channel_id=3, replica_groups=mesh['sp'=4,'tp'=8] {'sp'}, dimensions={0}, use_global_device_ids=true | all-gather | bytes 327680 | tf_op jit(solution)/shard_map/all_gather | solution.py:16
  170.0 1.1 while.41
  171.1 0.9 fusion.30
  172.0 8.3 %reduce-scatter.4.cloned.1.call-done = f32[512,2]{1,0:T(8,128)} async-done(((f32[4096,2]{1,0:T(8,128)}), f32[512,2]{1,0:T(8,128)}) %reduce-scatter.4.cloned.1.call-update) | async-done | bytes 4112
  180.3 1.6 copy.60
  (74 shorter events, 9.2 us)
Async XLA Ops:
  7.2 4.6 %copy-start = (bf16[4096,128]{1,0:T(8,128)(2,1)S(1)}, bf16[4096,128]{1,0:T(8,128)(2,1)}, u32[]{:S(2)}) copy-start(bf16[4096,128]{1,0:T(8,128)(2,1)} %param.20) | copy-start | bytes 3145732
  7.2 46.2 %copy-start.3 = (f32[2,256,1]{1,2,0:T(1,128)S(1)}, f32[2,256,1]{1,2,0:T(1,128)}, u32[]{:S(2)}) copy-start(f32[2,256,1]{1,2,0:T(1,128)} %param.27) | copy-start | bytes 6148
  7.2 42.8 %all-gather.5.cloned.1.call-start = ((), (), s32[]{:S(2)}) async-start(), calls=%async_computation.1 | async-start | bytes 4718592 | tf_op jit(solution)/shard_map/all_gather | solution.py:126
  7.9 172.3 %reduce-scatter.4.cloned.1.call-start = ((), (), s32[]{:S(2)}) async-start(), calls=%async_computation.2 | async-start | bytes 2359296
  54.1 44.4 %copy-start.5 = (bf16[4096,128]{1,0:T(8,128)(2,1)S(1)}, bf16[4096,128]{1,0:T(8,128)(2,1)}, u32[]{:S(2)}) copy-start(bf16[4096,128]{1,0:T(8,128)(2,1)} %param.21) | copy-start | bytes 3145732
  106.1 30.8 %copy-start.2 = (bf16[2,4096]{1,0:T(2,128)(2,1)S(1)}, bf16[2,4096]{1,0:T(2,128)(2,1)}, u32[]{:S(2)}) copy-start(bf16[2,4096]{1,0:T(2,128)(2,1)} %param.19) | copy-start | bytes 49156
  106.1 32.4 %copy-start.1 = (bf16[128,4096]{1,0:T(8,128)(2,1)S(1)}, bf16[128,4096]{1,0:T(8,128)(2,1)}, u32[]{:S(2)}) copy-start(bf16[128,4096]{1,0:T(8,128)(2,1)} %param.29) | copy-start | bytes 3145732
  106.1 32.4 %copy-start.4 = (f32[128]{0:T(128)S(1)}, f32[128]{0:T(128)}, u32[]{:S(2)}) copy-start(f32[128]{0:T(128)} %param.28) | copy-start | bytes 1540
Sparse Core Ops, SparseCore 0:
  9.9 40.0 all-gather.4
  141.9 38.3 reduce-scatter.3
where the time goes:
time: 189 us
  blocking collectives  56.6 us (30%)
  waiting for transfers between devices  43.9 us (23%)
  other arithmetic  41.5 us (22%)
  matrix products  26.6 us (14%)
  between operations  15 us (8%)
  local copies, waits for them, and re-layouts  4.71 us (2%)
    another operation x1, other arithmetic, segment_map(): lax.linalg.triangular_solve(system, targets, left_side=True, lower=True)  39.3 us
    all_gather x1, waiting for transfers between devices, body(): portion = lax.all_gather(context_activations, 'tp', axis=2, tiled=True)  34.9 us
    all_gather x2, blocking collectives, carried_in(): lax.all_gather(part.astype(kind), axis)  28.2 us
    all_gather x1, blocking collectives, carried_in_2(): everything = lax.all_gather(value, axis)  16.2 us
    psum x1, blocking collectives, body(): read = lax.psum(term, 'sp') + own_write  12.1 us
    unnamed x3, waiting for transfers between devices  8.97 us
  transfers between devices with their start and end apart: 2, of which 2 were waited for; matrix products, arithmetic and copies ran while one was open for 4% of the time, Pallas kernels for 0%

commit v1 on v0

v1 whole, which is shorter than its diff:
```python
import functools

import jax
import jax.numpy as jnp
from jax import lax
from jax.experimental import pallas as pl
from jax.experimental.pallas import tpu as pltpu
from jax.sharding import PartitionSpec as P

EPS = 1e-06
BF = jnp.bfloat16
F32 = jnp.float32
MESH = pl.DeviceIdType.MESH


def mm(a, b, dims=((1,), (0,))):
    return lax.dot_general(a, b, (dims, ((), ())), preferred_element_type=F32)


def split(a):
    hi = a.astype(BF)
    return hi, (a - hi.astype(F32)).astype(BF)


def mm_split_left(a, b, dims=((1,), (0,))):
    hi, lo = split(a)
    return mm(hi, b, dims) + mm(lo, b, dims)


def mm_split_right(a, b):
    hi, lo = split(b)
    return mm(a, hi) + mm(a, lo)


def mm3(a, b):
    ah, al = split(a)
    bh, bl = split(b)
    return mm(ah, bh) + (mm(ah, bl) + mm(al, bh))


def silu(v):
    return v / (1.0 + jnp.exp(-v))


def sigmoid(v):
    return 1.0 / (1.0 + jnp.exp(-v))


def softplus(v):
    return jnp.maximum(v, 0.0) + jnp.log1p(jnp.exp(-jnp.abs(v)))


def unit(v):
    return v * lax.rsqrt(jnp.sum(v * v, axis=-1, keepdims=True) + EPS)


def to_col(row, eye):
    return jnp.sum(jnp.where(eye, row, 0.0), axis=1, keepdims=True)


def to_row(col, eye):
    return jnp.sum(jnp.where(eye, col, 0.0), axis=0, keepdims=True)


def local_maps(keys, values, beta, log_decay, extra):
    n = keys[0].shape[0]
    i = lax.broadcasted_iota(jnp.int32, (n, n), 0)
    j = lax.broadcasted_iota(jnp.int32, (n, n), 1)
    eye = i == j
    blocks = range(len(keys))
    rows, cols, systems, solved = [], [], [], []
    for b in blocks:
        fade = log_decay[b] + to_col(extra[b], eye)
        c_row = jnp.sum(jnp.where(i <= j, fade, 0.0), axis=0, keepdims=True)
        c_col = to_col(c_row, eye)
        gram = mm(keys[b], keys[b], ((1,), (1,)))
        within = jnp.exp(jnp.where(i > j, c_col - c_row, 0.0))
        systems.append(jnp.where(i > j, beta[b] * gram * within, 0.0))
        rows.append(c_row)
        cols.append(c_col)
    for b in blocks:
        solved.append(
            jnp.where(eye, 1.0, 0.0) - jnp.where((i // 2) == (j // 2), systems[b], 0.0)
        )
    size = 2
    while size < n:
        mask = ((i // (2 * size)) == (j // (2 * size))) & ((i // size) != (j // size))
        half = [mm3(jnp.where(mask, systems[b], 0.0), solved[b]) for b in blocks]
        solved = [solved[b] - mm3(solved[b], half[b]) for b in blocks]
        size *= 2
    total = None
    for b in blocks:
        beta_row = to_row(beta[b], eye)
        scaled = solved[b] * beta_row
        pseudo = mm_split_left(scaled, values[b])
        decayed = mm_split_left(scaled * jnp.exp(rows[b]), keys[b])
        last = cols[b][n - 1 : n, :]
        trail = jnp.exp(last - cols[b])
        both = jnp.concatenate([-decayed, pseudo], axis=1) * trail
        hi, lo = split(both)
        turned = ((0,), (0,))
        both = mm(keys[b], hi, turned) + mm(keys[b], lo, turned)
        width = keys[b].shape[1]
        wi = lax.broadcasted_iota(jnp.int32, (width, both.shape[1]), 0)
        wj = lax.broadcasted_iota(jnp.int32, (width, both.shape[1]), 1)
        both = both + jnp.where(wi == wj, jnp.exp(last), 0.0)
        if total is None:
            total = both
        else:
            width_off = jnp.where(wj >= width, both, 0.0)
            total = mm3(both[:, :width], total) + width_off
    return total


def kernel(
    n_sp,
    n_tp,
    block,
    ctx,
    first,
    wk_hbm,
    wv_hbm,
    wq_hbm,
    wz_hbm,
    wlog,
    speeds,
    extra,
    gain,
    exit_hbm,
    state_out,
    step_out,
    buf,
    wkv,
    wqz,
    wexit,
    acc,
    lacc,
    maps,
    prev,
    msg_out,
    msg_in,
    read_out,
    read_in,
    part,
    parts,
    local_sem,
    send_sem,
    recv_sem,
    chain_send,
    chain_recv,
    back_send,
    back_recv,
    read_send,
    read_recv,
    part_send,
    part_recv,
):
    prompts, length, feats = ctx.shape
    head = wk_hbm.shape[1]
    sp = lax.axis_index("sp")
    tp = lax.axis_index("tp")
    pairs = [(wk_hbm, wkv, 0), (wv_hbm, wkv, 1), (wq_hbm, wqz, 0), (wz_hbm, wqz, 1)]
    loads = [
        pltpu.make_async_copy(src, dst.at[:, pl.ds(at * head, head)], local_sem.at[k])
        for k, (src, dst, at) in enumerate(pairs)
    ]
    loads.append(pltpu.make_async_copy(exit_hbm, wexit, local_sem.at[4]))
    loads.append(pltpu.make_async_copy(ctx, buf.at[tp], local_sem.at[5]))
    loads[5].start()
    for copy in loads[:5]:
        copy.start()

    barrier = pltpu.get_barrier_semaphore()
    for d in range(1, n_tp):
        pl.semaphore_signal(
            barrier, inc=1, device_id=(sp, lax.rem(tp + d, n_tp)), device_id_type=MESH
        )
    for d in range(1, n_sp):
        pl.semaphore_signal(
            barrier, inc=1, device_id=(lax.rem(sp + d, n_sp), tp), device_id_type=MESH
        )
    pl.semaphore_wait(barrier, n_tp + n_sp - 2)

    def gather_copy(source, p, target, k, from_input=False):
        return pltpu.make_async_remote_copy(
            src_ref=ctx.at[p] if from_input else buf.at[source, p],
            dst_ref=buf.at[source, p],
            send_sem=send_sem.at[k, p],
            recv_sem=recv_sem.at[source, p],
            device_id=(sp, target),
            device_id_type=MESH,
        )

    sends = []

    def go(copy):
        copy.start()
        sends.append(copy)

    def arrived(source, p):
        gather_copy(source, p, tp, 0).wait_recv()

    cube = n_tp == 8
    if cube:
        y, x, core = tp // 4, (tp // 2) % 2, tp % 2

        def at(yy, xx, cc):
            return yy * 4 + xx * 2 + cc

        def turn(yy, xx, cc, first_axis):
            on_x = (1 - cc) if first_axis else cc
            on_y = cc if first_axis else (1 - cc)
            return yy + on_y * (1 - 2 * yy), xx + on_x * (1 - 2 * xx)

        near = at(*turn(y, x, core, True), core)
        far = at(*turn(y, x, core, False), core)
        across = at(1 - y, 1 - x, core)
        partner = at(y, x, 1 - core)
        near2 = at(*turn(y, x, 1 - core, True), 1 - core)
        far2 = at(*turn(y, x, 1 - core, False), 1 - core)
        across2 = at(1 - y, 1 - x, 1 - core)
        for p in range(prompts):
            go(gather_copy(tp, p, near, 0, True))
            go(gather_copy(tp, p, far, 1, True))
            go(gather_copy(tp, p, partner, 2, True))
    else:
        for p in range(prompts):
            for d in range(1, n_tp):
                go(gather_copy(tp, p, lax.rem(tp + d, n_tp), d, True))

    for copy in loads[:4]:
        copy.wait()
    x1 = first[...]
    kv1 = mm(x1, wkv[...])
    qz1 = mm(x1, wqz[...])
    l1 = mm(x1, wlog[...])
    k1 = unit(silu(kv1[:, :head]))
    v1 = silu(kv1[:, head:])
    q1 = unit(silu(qz1[:, :head]))
    gate1 = silu(qz1[:, head:])
    heads = wlog.shape[1] // 2
    lanes = lax.broadcasted_iota(jnp.int32, (1, 2 * heads), 1)
    is_beta = lanes == tp
    is_decay = lanes == tp + heads
    speed_lanes = lax.broadcasted_iota(jnp.int32, (1, heads), 1)
    speed = jnp.sum(
        jnp.where(speed_lanes == tp, speeds[...], 0.0), axis=1, keepdims=True
    )

    def pick(logits, which):
        return jnp.sum(jnp.where(which, logits, 0.0), axis=1, keepdims=True)

    b1 = sigmoid(pick(l1, is_beta))
    a1 = jnp.exp(-speed * softplus(pick(l1, is_decay)))
    kq = jnp.sum(k1 * q1, axis=-1, keepdims=True)
    query = a1 * (q1 - b1 * k1 * kq)
    own_write = b1 * v1 * kq

    loads[5].wait()

    def project(source, p, fresh=False):
        xs = buf[source, p]
        at_row = pl.ds(pl.multiple_of(source * feats, feats), feats)
        kv = mm(xs, wkv[at_row, :])
        lg = mm(xs, wlog[at_row, :])
        if fresh:
            acc[p] = kv
            lacc[p] = lg
        else:
            acc[p] += kv
            lacc[p] += lg

    for p in range(prompts):
        project(tp, p, True)
        if cube:
            arrived(near, p)
            go(gather_copy(near, p, far, 3))
            go(gather_copy(near, p, partner, 4))
            arrived(far, p)
            go(gather_copy(far, p, partner, 5))
            arrived(partner, p)
            project(partner, p)
            project(near, p)
            project(far, p)
            arrived(near2, p)
            project(near2, p)
            arrived(far2, p)
            project(far2, p)
            arrived(across, p)
            go(gather_copy(across, p, partner, 6))
            project(across, p)
            arrived(across2, p)
            project(across2, p)
        else:

            def one(d, carry):
                source = lax.rem(tp + d, n_tp)
                arrived(source, p)
                project(source, p)
                return carry

            lax.fori_loop(1, n_tp, one, 0)

        kv = acc[p]
        keys = unit(silu(kv[:, :head])).astype(BF)
        values = silu(kv[:, head:]).astype(BF)
        scores = lacc[p].astype(BF).astype(F32)
        beta = sigmoid(pick(scores, is_beta))
        fade = -speed * softplus(pick(scores, is_decay))
        cuts = [slice(b * block, (b + 1) * block) for b in range(length // block)]
        maps[p] = local_maps(
            [keys[c] for c in cuts],
            [values[c] for c in cuts],
            [beta[c] for c in cuts],
            [fade[c] for c in cuts],
            [extra[p : p + 1, c] for c in cuts],
        )

    hi_ = lax.broadcasted_iota(jnp.int32, (head, head), 0)
    hj_ = lax.broadcasted_iota(jnp.int32, (head, head), 1)
    heye = hi_ == hj_
    last_sp = n_sp - 1
    meet = max(n_sp // 2 - 1, 0)

    def chain_copy(p):
        return pltpu.make_async_remote_copy(
            src_ref=state_out.at[p],
            dst_ref=prev.at[p],
            send_sem=chain_send.at[p],
            recv_sem=chain_recv.at[p],
            device_id=(lax.rem(sp + 1, n_sp), tp),
            device_id_type=MESH,
        )

    def back_copy():
        return pltpu.make_async_remote_copy(
            src_ref=msg_out,
            dst_ref=msg_in,
            send_sem=back_send.at[0],
            recv_sem=back_recv.at[0],
            device_id=(lax.rem(sp + n_sp - 1, n_sp), tp),
            device_id_type=MESH,
        )

    def forward_first():
        for p in range(prompts):
            state_out[p] = maps[p][:, head:].astype(BF)
            if n_sp > 1:
                chain_copy(p).start()

    def forward_later(send):
        for p in range(prompts):
            chain_copy(p).wait_recv()
            both = maps[p]
            state = mm_split_left(both[:, :head], prev[p]) + both[:, head:]
            maps[p, :, head:] = state
            state_out[p] = state.astype(BF)
            if send:
                chain_copy(p).start()

    def back_step(message):
        for p in range(prompts):
            line = message[p : p + 1, :]
            col = to_col(line, heye)
            out = jnp.sum(col * maps[p], axis=0, keepdims=True)
            msg_out[p : p + 1, :] = out[:, :head]
            msg_out[prompts + p : prompts + p + 1, :] = (
                message[prompts + p : prompts + p + 1, :] + out[:, head:]
            )

    pl.when(sp == 0)(forward_first)
    if n_sp > 1:

        @pl.when(sp == last_sp)
        def _():
            back_step(jnp.concatenate([query, jnp.zeros_like(query)], axis=0))
            back_copy().start()

        if last_sp - meet > 1:

            @pl.when((sp > meet) & (sp < last_sp))
            def _():
                back_copy().wait_recv()
                back_step(msg_in[...])
                back_copy().start()

        if n_sp > 2:

            @pl.when((sp > 0) & (sp < last_sp))
            def _():
                forward_later(True)

    def read_copy(d, mine):
        return pltpu.make_async_remote_copy(
            src_ref=read_out,
            dst_ref=read_in,
            send_sem=read_send.at[d],
            recv_sem=read_recv.at[0],
            device_id=(lax.rem(sp + d, n_sp), tp),
            device_id_type=MESH,
        )

    @pl.when(sp == meet)
    def _():
        if n_sp > 1:
            back_copy().wait_recv()
            message = msg_in[...]
        else:
            message = jnp.concatenate([query, jnp.zeros_like(query)], axis=0)
        for p in range(prompts):
            col = to_col(message[p : p + 1, :], heye)
            out = jnp.sum(col * maps[p, :, head:], axis=0, keepdims=True)
            read = message[prompts + p : prompts + p + 1, :] + out
            read_out[p : p + 1, :] = read + own_write[p : p + 1, :]
        for d in range(1, n_sp):
            read_copy(d, True).start()
        read_in[...] = read_out[...]

    if n_sp > 1:

        @pl.when(sp != meet)
        def _():
            read_copy(0, False).wait_recv()

    read = read_in[...]
    normed = (
        read
        * lax.rsqrt(jnp.mean(read * read, axis=-1, keepdims=True) + EPS)
        * gain[...]
        * gate1
    ).astype(BF)
    loads[4].wait()
    shares = mm(normed, wexit[...])
    width = step_out.shape[1]
    for t in range(n_tp):
        part[t] = shares[:, t * width : (t + 1) * width]

    def part_copy(d):
        target = lax.rem(tp + d, n_tp)
        return pltpu.make_async_remote_copy(
            src_ref=part.at[target],
            dst_ref=parts.at[tp],
            send_sem=part_send.at[d],
            recv_sem=part_recv.at[tp],
            device_id=(sp, target),
            device_id_type=MESH,
        )

    def part_arrived(source):
        return pltpu.make_async_remote_copy(
            src_ref=part.at[0],
            dst_ref=parts.at[source],
            send_sem=part_send.at[0],
            recv_sem=part_recv.at[source],
            device_id=(sp, tp),
            device_id_type=MESH,
        )

    for d in range(1, n_tp):
        part_copy(d).start()
    parts[tp] = part[tp]

    if n_sp > 1:

        @pl.when(sp == last_sp)
        def _():
            forward_later(False)

    for d in range(1, n_tp):
        part_arrived(lax.rem(tp + d, n_tp)).wait_recv()
    total = parts[0]
    for t in range(1, n_tp):
        total = total + parts[t]
    step_out[...] = total.astype(BF)

    for copy in sends:
        copy.wait_send()
    for d in range(1, n_tp):
        part_copy(d).wait_send()
    if n_sp > 1:

        @pl.when(sp < last_sp)
        def _():
            for p in range(prompts):
                chain_copy(p).wait_send()

        @pl.when(sp > meet)
        def _():
            back_copy().wait_send()

        @pl.when(sp == meet)
        def _():
            for d in range(1, n_sp):
                read_copy(d, True).wait_send()


def body(
    n_sp,
    n_tp,
    context,
    first,
    wk,
    wv,
    wq,
    wz,
    w_write,
    w_fade,
    speeds,
    extra,
    gain,
    w_exit,
):
    head = gain.shape[0]
    prompts, length, feats = context.shape
    width = wk.shape[0]
    heads = w_write.shape[1]
    assert wk.shape[1] == head and heads == n_tp
    block = min(head, length)
    wlog = jnp.concatenate([w_write, w_fade], axis=1)
    vmem = pl.BlockSpec(memory_space=pltpu.VMEM)
    anym = pl.BlockSpec(memory_space=pl.ANY)
    dma = pltpu.SemaphoreType.DMA
    out_cols = w_exit.shape[1] // n_tp
    state, step = pl.pallas_call(
        functools.partial(kernel, n_sp, n_tp, block),
        name="delta",
        out_shape=(
            jax.ShapeDtypeStruct((prompts, head, head), BF),
            jax.ShapeDtypeStruct((prompts, out_cols), BF),
        ),
        in_specs=[anym, vmem, anym, anym, anym, anym, vmem, vmem, vmem, vmem, anym],
        out_specs=(vmem, vmem),
        scratch_shapes=[
            pltpu.VMEM((n_tp, prompts, length, feats), BF),
            pltpu.VMEM((width, 2 * head), BF),
            pltpu.VMEM((width, 2 * head), BF),
            pltpu.VMEM(w_exit.shape, BF),
            pltpu.VMEM((prompts, length, 2 * head), F32),
            pltpu.VMEM((prompts, length, 2 * heads), F32),
            pltpu.VMEM((prompts, head, 2 * head), F32),
            pltpu.VMEM((prompts, head, head), BF),
            pltpu.VMEM((2 * prompts, head), F32),
            pltpu.VMEM((2 * prompts, head), F32),
            pltpu.VMEM((prompts, head), F32),
            pltpu.VMEM((prompts, head), F32),
            pltpu.VMEM((n_tp, prompts, out_cols), F32),
            pltpu.VMEM((n_tp, prompts, out_cols), F32),
            dma((6,)),
            dma((max(n_tp, 7), prompts)),
            dma((n_tp, prompts)),
            dma((prompts,)),
            dma((prompts,)),
            dma((1,)),
            dma((1,)),
            dma((n_sp,)),
            dma((1,)),
            dma((n_tp,)),
            dma((n_tp,)),
        ],
        compiler_params=pltpu.CompilerParams(
            collective_id=0, has_side_effects=True, vmem_limit_bytes=60 * 2**20
        ),
    )(
        context,
        first,
        wk,
        wv,
        wq,
        wz,
        wlog,
        speeds.reshape(1, heads),
        extra.reshape(prompts, length),
        gain.reshape(1, head),
        w_exit,
    )
    return state[:, None, None], step


def solution(mesh):
    placed = (
        P(None, "sp", "tp"),
        P(),
        P(None, "tp"),
        P(None, "tp"),
        P(None, "tp"),
        P(None, "tp"),
        P(),
        P(),
        P(),
        P(None, "sp", "tp"),
        P(),
        P("tp", None),
    )
    return jax.shard_map(
        functools.partial(body, mesh.shape["sp"], mesh.shape["tp"]),
        mesh=mesh,
        in_specs=placed,
        out_specs=(P(None, "sp", "tp", None, None), P(None, "tp")),
        check_vma=False,
    )
```

time: 189 us -> 55.6 us (0.29)
  blocking collectives: 56.6 us -> 0 us
  Pallas kernels: 0 us -> 49.9 us
  waiting for transfers between devices: 43.9 us -> 0 us
  other arithmetic: 41.5 us -> 0.88 us
  matrix products: 26.6 us -> 0 us
  between operations: 15 us -> 0.66 us
    pallas_call x0 -> x1, Pallas kernels: none -> 49.9 us  [body(): pl.pallas_call(functools.partial(kernel, n_sp, n_tp, block), name='delta'...]
    all_gather x3 -> x0, blocking collectives: 44.4 us -> none  [the longest x2 28.2 us: carried_in(): lax.all_gather(part.astype(kind), axis)]
    another operation x2 -> x0, other arithmetic: 39.8 us -> none  [the longest x1 39.3 us: segment_map(): lax.linalg.triangular_solve(system, targets, left_side=True, lower=True)]
    all_gather x1 -> x0, waiting for transfers between devices: 34.9 us -> none  [body(): portion = lax.all_gather(context_activations, 'tp', axis=2, tiled=True)]
    dot_general x27 -> x0, matrix products: 22.7 us -> none  [the longest x1 3.55 us: body(): jnp.einsum('abf,fc->abc', portion, address_projection, preferred_element_...]
    psum x1 -> x0, blocking collectives: 12.1 us -> none  [body(): read = lax.psum(term, 'sp') + own_write]
    unnamed x3 -> x0, waiting for transfers between devices: 8.97 us -> none
    unnamed x1 -> x0, matrix products: 3.27 us -> none
  transfers between devices with their start and end apart: 2 -> 0, of which waited for: 2 -> 0; matrix products, arithmetic and copies ran while one was open for 4% -> 0% of each run, Pallas kernels for 0% -> 0%
where the time goes in v1:
time: 55.6 us; the launch traced here: 55.4 us
  Pallas kernels  49.9 us (90%)
  local copies, waits for them, and re-layouts  3.96 us (7%)
  other arithmetic  0.88 us (2%)
  between operations  0.66 us (1%)
    pallas_call x1, Pallas kernels, body(): pl.pallas_call(functools.partial(kernel, n_sp, n_tp, block), name='delta'...  49.9 us
    unnamed x7, local copies, waits for them, and re-layouts  2.64 us
    concatenate x1, local copies, waits for them, and re-layouts, body(): wlog = jnp.concatenate([w_write, w_fade], axis=1)  1.32 us

profile of v1, /device:TPU:0, one launch (start us, length us, event | category | flops | bytes accessed | tf_op | source)
XLA Modules:
  0.0 55.4 jit_solution(8210904452008394543)
XLA Ops:
  0.6 0.9 %pad_maximum_fusion = bf16[4096,16]{0,1:T(8,128)(2,1)S(1)} fusion(bf16[4096,8]{0,1:T(8,128)(2,1)} %param.19, bf16[4096,8]{0,1:T(8,128)(2,1)} %param.18), kind=kLoop, calls=%fused_computation | loop fusion | flops 262144 | bytes 262144 | tf_op jit(solution)/shard_map/concatenate | solution.py:519
  1.5 0.0 copy-start
  1.5 1.3 %copy.17.wlog = bf16[4096,16]{1,0:T(8,128)(2,1)} copy(bf16[4096,16]{0,1:T(8,128)(2,1)S(1)} %pad_maximum_fusion) | data formatting | bytes 262144 | tf_op jit(solution)/shard_map/concatenate | solution.py:519
  2.8 0.0 copy-done
  2.8 0.6 %copy.21 = f32[2,256,1]{1,0,2:T(2,128)} copy(f32[2,256,1]{1,2,0:T(1,128)S(1)} %copy-done) | data formatting | bytes 4096
  3.4 49.9 %delta.1 = (bf16[2,128,128]{2,1,0:T(8,128)(2,1)}, bf16[2,512]{1,0:T(2,128)(2,1)}) custom-call(bf16[2,256,512]{2,1,0:T(8,128)(2,1)} %ctx.1, bf16[2,4096]{1,0:T(2,128)(2,1)} %first.1, bf16[4096,128]{1,0:T(8,128)(2,1)} %wk_hbm.1, bf16[4096,128]{1,0:T(8,128)(2,1)} %wv_hbm.1, bf16[4096,128]{1,0:T(8,128)(2,1)} %wq_hbm.1, bf16[4096,128]{1,0:T(8,128)(2,1)} %wz_hbm.1, ...), custom_call_target="tpu_custom_call" | custom-call | tf_op jit(solution)/shard_map/delta/pallas_call | solution.py:524
  53.3 0.0 copy-start.1
  53.3 1.5 %copy.24 = bf16[2,1,1,128,128]{4,3,2,1,0:T(8,128)(2,1)} copy(bf16[2,1,1,128,128]{4,3,2,1,0:T(8,128)(2,1)} %bitcast.8) | data formatting | bytes 131072
  54.8 0.0 copy-done.1
  54.8 0.6 %copy.25 = bf16[2,512]{1,0:T(2,128)(2,1)} copy(bf16[2,512]{1,0:T(2,128)(2,1)S(1)} %copy-done.1) | data formatting | bytes 4096
Async XLA Ops:
  1.5 1.3 %copy-start = (f32[2,256,1]{1,2,0:T(1,128)S(1)}, f32[2,256,1]{1,2,0:T(1,128)}, u32[]{:S(2)}) copy-start(f32[2,256,1]{1,2,0:T(1,128)} %param.21) | copy-start | bytes 6148
  53.3 1.5 %copy-start.1 = (bf16[2,512]{1,0:T(2,128)(2,1)S(1)}, bf16[2,512]{1,0:T(2,128)(2,1)}, u32[]{:S(2)}) copy-start(bf16[2,512]{1,0:T(2,128)(2,1)} %get-tuple-element.13) | copy-start | bytes 6148

commit v2 on v1

--- a/solution.py
+++ b/solution.py
@@ -122,7 +122,8 @@
     wv_hbm,
     wq_hbm,
     wz_hbm,
-    wlog,
+    w_write,
+    w_fade,
     speeds,
     extra,
     gain,
@@ -134,8 +135,10 @@
     wqz,
     wexit,
     acc,
-    lacc,
+    bacc,
+    facc,
     maps,
+    sent,
     prev,
     msg_out,
     msg_in,
@@ -179,11 +182,12 @@
         pl.semaphore_signal(
             barrier, inc=1, device_id=(lax.rem(sp + d, n_sp), tp), device_id_type=MESH
         )
+    loads[5].wait()
     pl.semaphore_wait(barrier, n_tp + n_sp - 2)
 
-    def gather_copy(source, p, target, k, from_input=False):
+    def gather_copy(source, p, target, k):
         return pltpu.make_async_remote_copy(
-            src_ref=ctx.at[p] if from_input else buf.at[source, p],
+            src_ref=buf.at[source, p],
             dst_ref=buf.at[source, p],
             send_sem=send_sem.at[k, p],
             recv_sem=recv_sem.at[source, p],
@@ -220,61 +224,115 @@
         far2 = at(*turn(y, x, 1 - core, False), 1 - core)
         across2 = at(1 - y, 1 - x, 1 - core)
         for p in range(prompts):
-            go(gather_copy(tp, p, near, 0, True))
-            go(gather_copy(tp, p, far, 1, True))
-            go(gather_copy(tp, p, partner, 2, True))
+            go(gather_copy(tp, p, near, 0))
+            if p == 0:
+                go(gather_copy(tp, p, far, 1))
+            go(gather_copy(tp, p, partner, 2))
     else:
         for p in range(prompts):
             for d in range(1, n_tp):
-                go(gather_copy(tp, p, lax.rem(tp + d, n_tp), d, True))
+                go(gather_copy(tp, p, lax.rem(tp + d, n_tp), d))
 
     for copy in loads[:4]:
         copy.wait()
     x1 = first[...]
     kv1 = mm(x1, wkv[...])
     qz1 = mm(x1, wqz[...])
-    l1 = mm(x1, wlog[...])
+    turned = ((1,), (1,))
+    lb1 = mm(x1, w_write[...], turned)
+    lf1 = mm(x1, w_fade[...], turned)
     k1 = unit(silu(kv1[:, :head]))
     v1 = silu(kv1[:, head:])
     q1 = unit(silu(qz1[:, :head]))
     gate1 = silu(qz1[:, head:])
-    heads = wlog.shape[1] // 2
-    lanes = lax.broadcasted_iota(jnp.int32, (1, 2 * heads), 1)
-    is_beta = lanes == tp
-    is_decay = lanes == tp + heads
-    speed_lanes = lax.broadcasted_iota(jnp.int32, (1, heads), 1)
-    speed = jnp.sum(
-        jnp.where(speed_lanes == tp, speeds[...], 0.0), axis=1, keepdims=True
-    )
-
-    def pick(logits, which):
-        return jnp.sum(jnp.where(which, logits, 0.0), axis=1, keepdims=True)
-
-    b1 = sigmoid(pick(l1, is_beta))
-    a1 = jnp.exp(-speed * softplus(pick(l1, is_decay)))
+    heads = w_write.shape[0]
+    mine = lax.broadcasted_iota(jnp.int32, (1, heads), 1) == tp
+
+    def pick(logits):
+        return jnp.sum(jnp.where(mine, logits, 0.0), axis=1, keepdims=True)
+
+    speed = pick(speeds[...])
+    b1 = sigmoid(pick(lb1))
+    a1 = jnp.exp(-speed * softplus(pick(lf1)))
     kq = jnp.sum(k1 * q1, axis=-1, keepdims=True)
     query = a1 * (q1 - b1 * k1 * kq)
     own_write = b1 * v1 * kq
-
-    loads[5].wait()
 
     def project(source, p, fresh=False):
         xs = buf[source, p]
         at_row = pl.ds(pl.multiple_of(source * feats, feats), feats)
         kv = mm(xs, wkv[at_row, :])
-        lg = mm(xs, wlog[at_row, :])
+        lb = mm(xs, w_write[:, at_row], turned)
+        lf = mm(xs, w_fade[:, at_row], turned)
         if fresh:
             acc[p] = kv
-            lacc[p] = lg
+            bacc[p] = lb
+            facc[p] = lf
         else:
             acc[p] += kv
-            lacc[p] += lg
+            bacc[p] += lb
+            facc[p] += lf
+
+    hi_ = lax.broadcasted_iota(jnp.int32, (head, head), 0)
+    hj_ = lax.broadcasted_iota(jnp.int32, (head, head), 1)
+    heye = hi_ == hj_
+    last_sp = n_sp - 1
+    meet = max(n_sp // 2 - 1, 0)
+
+    def chain_copy(p):
+        return pltpu.make_async_remote_copy(
+            src_ref=sent.at[p],
+            dst_ref=prev.at[p],
+            send_sem=chain_send.at[p],
+            recv_sem=chain_recv.at[p],
+            device_id=(lax.rem(sp + 1, n_sp), tp),
+            device_id_type=MESH,
+        )
+
+    def back_copy():
+        return pltpu.make_async_remote_copy(
+            src_ref=msg_out,
+            dst_ref=msg_in,
+            send_sem=back_send.at[0],
+            recv_sem=back_recv.at[0],
+            device_id=(lax.rem(sp + n_sp - 1, n_sp), tp),
+            device_id_type=MESH,
+        )
+
+    def forward_first(p):
+        state_out[p] = maps[p, :, head:]
+        sent[p] = maps[p, :, head:].astype(BF)
+        if n_sp > 1:
+            chain_copy(p).start()
+
+    def forward_later(send):
+        for p in range(prompts):
+            chain_copy(p).wait_recv()
+            both = maps[p]
+            state = mm_split_left(both[:, :head], prev[p]) + both[:, head:]
+            maps[p, :, head:] = state
+            state_out[p] = state
+            if send:
+                sent[p] = state.astype(BF)
+                chain_copy(p).start()
+
+    def back_step(message):
+        for p in range(prompts):
+            line = message[p : p + 1, :]
+            col = to_col(line, heye)
+            out = jnp.sum(col * maps[p], axis=0, keepdims=True)
+            msg_out[p : p + 1, :] = out[:, :head]
+            msg_out[prompts + p : prompts + p + 1, :] = (
+                message[prompts + p : prompts + p + 1, :] + out[:, head:]
+            )
 
     for p in range(prompts):
         project(tp, p, True)
         if cube:
             arrived(near, p)
             go(gather_copy(near, p, far, 3))
+            if p + 1 < prompts:
+                go(gather_copy(tp, p + 1, far, 1))
             go(gather_copy(near, p, partner, 4))
             arrived(far, p)
             go(gather_copy(far, p, partner, 5))
@@ -304,71 +362,18 @@
         kv = acc[p]
         keys = unit(silu(kv[:, :head])).astype(BF)
         values = silu(kv[:, head:]).astype(BF)
-        scores = lacc[p].astype(BF).astype(F32)
-        beta = sigmoid(pick(scores, is_beta))
-        fade = -speed * softplus(pick(scores, is_decay))
+        beta = sigmoid(pick(bacc[p].astype(BF).astype(F32)))
+        fade = -speed * softplus(pick(facc[p].astype(BF).astype(F32)))
         cuts = [slice(b * block, (b + 1) * block) for b in range(length // block)]
         maps[p] = local_maps(
             [keys[c] for c in cuts],
             [values[c] for c in cuts],
             [beta[c] for c in cuts],
             [fade[c] for c in cuts],
-            [extra[p : p + 1, c] for c in cuts],
-        )
-
-    hi_ = lax.broadcasted_iota(jnp.int32, (head, head), 0)
-    hj_ = lax.broadcasted_iota(jnp.int32, (head, head), 1)
-    heye = hi_ == hj_
-    last_sp = n_sp - 1
-    meet = max(n_sp // 2 - 1, 0)
-
-    def chain_copy(p):
-        return pltpu.make_async_remote_copy(
-            src_ref=state_out.at[p],
-            dst_ref=prev.at[p],
-            send_sem=chain_send.at[p],
-            recv_sem=chain_recv.at[p],
-            device_id=(lax.rem(sp + 1, n_sp), tp),
-            device_id_type=MESH,
-        )
-
-    def back_copy():
-        return pltpu.make_async_remote_copy(
-            src_ref=msg_out,
-            dst_ref=msg_in,
-            send_sem=back_send.at[0],
-            recv_sem=back_recv.at[0],
-            device_id=(lax.rem(sp + n_sp - 1, n_sp), tp),
-            device_id_type=MESH,
-        )
-
-    def forward_first():
-        for p in range(prompts):
-            state_out[p] = maps[p][:, head:].astype(BF)
-            if n_sp > 1:
-                chain_copy(p).start()
-
-    def forward_later(send):
-        for p in range(prompts):
-            chain_copy(p).wait_recv()
-            both = maps[p]
-            state = mm_split_left(both[:, :head], prev[p]) + both[:, head:]
-            maps[p, :, head:] = state
-            state_out[p] = state.astype(BF)
-            if send:
-                chain_copy(p).start()
-
-    def back_step(message):
-        for p in range(prompts):
-            line = message[p : p + 1, :]
-            col = to_col(line, heye)
-            out = jnp.sum(col * maps[p], axis=0, keepdims=True)
-            msg_out[p : p + 1, :] = out[:, :head]
-            msg_out[prompts + p : prompts + p + 1, :] = (
-                message[prompts + p : prompts + p + 1, :] + out[:, head:]
-            )
-
-    pl.when(sp == 0)(forward_first)
+            [extra[p, :, c] for c in cuts],
+        )
+        pl.when(sp == 0)(functools.partial(forward_first, p))
+
     if n_sp > 1:
 
         @pl.when(sp == last_sp)
@@ -471,7 +476,7 @@
     total = parts[0]
     for t in range(1, n_tp):
         total = total + parts[t]
-    step_out[...] = total.astype(BF)
+    step_out[...] = total
 
     for copy in sends:
         copy.wait_send()
@@ -516,7 +521,6 @@
     heads = w_write.shape[1]
     assert wk.shape[1] == head and heads == n_tp
     block = min(head, length)
-    wlog = jnp.concatenate([w_write, w_fade], axis=1)
     vmem = pl.BlockSpec(memory_space=pltpu.VMEM)
     anym = pl.BlockSpec(memory_space=pl.ANY)
     dma = pltpu.SemaphoreType.DMA
@@ -525,10 +529,10 @@
         functools.partial(kernel, n_sp, n_tp, block),
         name="delta",
         out_shape=(
-            jax.ShapeDtypeStruct((prompts, head, head), BF),
-            jax.ShapeDtypeStruct((prompts, out_cols), BF),
+            jax.ShapeDtypeStruct((prompts, head, head), F32),
+            jax.ShapeDtypeStruct((prompts, out_cols), F32),
         ),
-        in_specs=[anym, vmem, anym, anym, anym, anym, vmem, vmem, vmem, vmem, anym],
+        in_specs=[anym, vmem] + [anym] * 4 + [vmem] * 5 + [anym],
         out_specs=(vmem, vmem),
         scratch_shapes=[
             pltpu.VMEM((n_tp, prompts, length, feats), BF),
@@ -536,8 +540,10 @@
             pltpu.VMEM((width, 2 * head), BF),
             pltpu.VMEM(w_exit.shape, BF),
             pltpu.VMEM((prompts, length, 2 * head), F32),
-            pltpu.VMEM((prompts, length, 2 * heads), F32),
+            pltpu.VMEM((prompts, length, heads), F32),
+            pltpu.VMEM((prompts, length, heads), F32),
             pltpu.VMEM((prompts, head, 2 * head), F32),
+            pltpu.VMEM((prompts, head, head), BF),
             pltpu.VMEM((prompts, head, head), BF),
             pltpu.VMEM((2 * prompts, head), F32),
             pltpu.VMEM((2 * prompts, head), F32),
@@ -558,7 +564,7 @@
             dma((n_tp,)),
         ],
         compiler_params=pltpu.CompilerParams(
-            collective_id=0, has_side_effects=True, vmem_limit_bytes=60 * 2**20
+            collective_id=0, has_side_effects=True, vmem_limit_bytes=64 * 2**20 - 420 * 2**10
         ),
     )(
         context,
@@ -567,13 +573,14 @@
         wv,
         wq,
         wz,
-        wlog,
+        w_write.T,
+        w_fade.T,
         speeds.reshape(1, heads),
-        extra.reshape(prompts, length),
+        extra.reshape(prompts, 1, length),
         gain.reshape(1, head),
         w_exit,
     )
-    return state[:, None, None], step
+    return state[:, None, None].astype(BF), step.astype(BF)
 
 
 def solution(mesh):

time: 55.6 us -> 49.8 us (0.90)
  local copies, waits for them, and re-layouts: 3.96 us -> 0.01 us
  Pallas kernels: 49.9 us -> 46.9 us
  other arithmetic: 0.88 us -> 2.12 us
    pallas_call x1, Pallas kernels: 49.9 us -> 46.9 us  [body(): pl.pallas_call(functools.partial(kernel, n_sp, n_tp, block), name='delta'...]
    unnamed x7 -> x2, local copies, waits for them, and re-layouts: 2.64 us -> 0.01 us
    unnamed x0 -> x1, other arithmetic: none -> 1.54 us
    concatenate x1 -> x0, local copies, waits for them, and re-layouts: 1.32 us -> none  [body(): wlog = jnp.concatenate([w_write, w_fade], axis=1)]
    concatenate x1 -> x0, other arithmetic: 0.88 us -> none  [body(): wlog = jnp.concatenate([w_write, w_fade], axis=1)]
    convert_element_type x0 -> x1, other arithmetic: none -> 0.58 us  [body(): return (state[:, None, None].astype(BF), step.astype(BF))]
where the time goes in v2:
time: 49.8 us; the launch traced here: 49.6 us
  Pallas kernels  46.9 us (94%)
  other arithmetic  2.12 us (4%)
  between operations  0.65 us (1%)
    pallas_call x1, Pallas kernels, body(): pl.pallas_call(functools.partial(kernel, n_sp, n_tp, block), name='delta'...  46.9 us
    unnamed x1, other arithmetic  1.54 us

profile of v2, /device:TPU:0, one launch (start us, length us, event | category | flops | bytes accessed | tf_op | source)
XLA Modules:
  0.0 49.6 jit_solution(14478835976591415992)
XLA Ops:
  0.6 46.9 %delta.1 = (f32[2,128,128]{2,1,0:T(8,128)}, f32[2,512]{1,0:T(2,128)}) custom-call(bf16[2,256,512]{2,1,0:T(8,128)(2,1)} %ctx.1, bf16[2,4096]{1,0:T(2,128)(2,1)} %first.1, bf16[4096,128]{1,0:T(8,128)(2,1)} %wk_hbm.1, bf16[4096,128]{1,0:T(8,128)(2,1)} %wv_hbm.1, bf16[4096,128]{1,0:T(8,128)(2,1)} %wq_hbm.1, bf16[4096,128]{1,0:T(8,128)(2,1)} %wz_hbm.1, ...), custom_call_target="tpu_custom_call" | custom-call | tf_op jit(solution)/shard_map/delta/pallas_call | solution.py:528
  47.5 0.0 copy-start
  47.5 1.5 %convert_bitcast_fusion = bf16[2,1,1,128,128]{4,3,2,1,0:T(8,128)(2,1)} fusion(f32[2,128,128]{2,1,0:T(8,128)} %get-tuple-element.4), kind=kLoop, calls=%fused_computation | loop fusion | flops 32768 | bytes 196608
  49.1 0.0 copy-done
  49.1 0.6 %convert_element_type.11 = bf16[2,512]{1,0:T(2,128)(2,1)} convert(f32[2,512]{1,0:T(2,128)S(1)} %copy-done) | non-fusion elementwise | flops 1024 | bytes 6144 | tf_op jit(solution)/shard_map/convert_element_type | solution.py:583
Async XLA Ops:
  47.5 1.6 %copy-start = (f32[2,512]{1,0:T(2,128)S(1)}, f32[2,512]{1,0:T(2,128)}, u32[]{:S(2)}) copy-start(f32[2,512]{1,0:T(2,128)} %get-tuple-element.5) | copy-start | bytes 12292

commit v3 on v2

--- a/solution.py
+++ b/solution.py
@@ -117,19 +117,25 @@
     n_tp,
     block,
     ctx,
-    first,
+    first_hbm,
     wk_hbm,
     wv_hbm,
     wq_hbm,
     wz_hbm,
+    write_hbm,
+    fade_hbm,
+    speeds_hbm,
+    extra_hbm,
+    gain_hbm,
+    exit_hbm,
+    state_out,
+    step_out,
+    first,
     w_write,
     w_fade,
     speeds,
     extra,
     gain,
-    exit_hbm,
-    state_out,
-    step_out,
     buf,
     wkv,
     wqz,
@@ -170,6 +176,20 @@
     loads.append(pltpu.make_async_copy(exit_hbm, wexit, local_sem.at[4]))
     loads.append(pltpu.make_async_copy(ctx, buf.at[tp], local_sem.at[5]))
     loads[5].start()
+    few = [
+        (first_hbm, first),
+        (write_hbm, w_write),
+        (fade_hbm, w_fade),
+        (speeds_hbm, speeds),
+        (extra_hbm, extra),
+        (gain_hbm, gain),
+    ]
+    small = [
+        pltpu.make_async_copy(src, dst, local_sem.at[6 + k])
+        for k, (src, dst) in enumerate(few)
+    ]
+    for copy in small:
+        copy.start()
     for copy in loads[:5]:
         copy.start()
 
@@ -233,7 +253,7 @@
             for d in range(1, n_tp):
                 go(gather_copy(tp, p, lax.rem(tp + d, n_tp), d))
 
-    for copy in loads[:4]:
+    for copy in loads[:4] + small:
         copy.wait()
     x1 = first[...]
     kv1 = mm(x1, wkv[...])
@@ -326,14 +346,18 @@
                 message[prompts + p : prompts + p + 1, :] + out[:, head:]
             )
 
+    def relay(p):
+        arrived(near, p)
+        go(gather_copy(near, p, far, 3))
+        if p + 1 < prompts:
+            go(gather_copy(tp, p + 1, far, 1))
+        go(gather_copy(near, p, partner, 4))
+
     for p in range(prompts):
         project(tp, p, True)
         if cube:
-            arrived(near, p)
-            go(gather_copy(near, p, far, 3))
-            if p + 1 < prompts:
-                go(gather_copy(tp, p + 1, far, 1))
-            go(gather_copy(near, p, partner, 4))
+            if p == 0:
+                relay(p)
             arrived(far, p)
             go(gather_copy(far, p, partner, 5))
             arrived(partner, p)
@@ -349,6 +373,8 @@
             project(across, p)
             arrived(across2, p)
             project(across2, p)
+            if p + 1 < prompts:
+                relay(p + 1)
         else:
 
             def one(d, carry):
@@ -522,19 +548,25 @@
     assert wk.shape[1] == head and heads == n_tp
     block = min(head, length)
     vmem = pl.BlockSpec(memory_space=pltpu.VMEM)
-    anym = pl.BlockSpec(memory_space=pl.ANY)
+    anym = pl.BlockSpec(memory_space=pltpu.HBM)
     dma = pltpu.SemaphoreType.DMA
     out_cols = w_exit.shape[1] // n_tp
     state, step = pl.pallas_call(
         functools.partial(kernel, n_sp, n_tp, block),
         name="delta",
         out_shape=(
-            jax.ShapeDtypeStruct((prompts, head, head), F32),
-            jax.ShapeDtypeStruct((prompts, out_cols), F32),
+            pltpu.VMEM((prompts, head, head), F32),
+            pltpu.VMEM((prompts, out_cols), F32),
         ),
-        in_specs=[anym, vmem] + [anym] * 4 + [vmem] * 5 + [anym],
+        in_specs=[anym] * 12,
         out_specs=(vmem, vmem),
         scratch_shapes=[
+            pltpu.VMEM(first.shape, BF),
+            pltpu.VMEM(w_write.shape[::-1], BF),
+            pltpu.VMEM(w_fade.shape[::-1], BF),
+            pltpu.VMEM((1, heads), F32),
+            pltpu.VMEM((prompts, 1, length), F32),
+            pltpu.VMEM((1, head), F32),
             pltpu.VMEM((n_tp, prompts, length, feats), BF),
             pltpu.VMEM((width, 2 * head), BF),
             pltpu.VMEM((width, 2 * head), BF),
@@ -551,7 +583,7 @@
             pltpu.VMEM((prompts, head), F32),
             pltpu.VMEM((n_tp, prompts, out_cols), F32),
             pltpu.VMEM((n_tp, prompts, out_cols), F32),
-            dma((6,)),
+            dma((12,)),
             dma((max(n_tp, 7), prompts)),
             dma((n_tp, prompts)),
             dma((prompts,)),
@@ -564,7 +596,7 @@
             dma((n_tp,)),
         ],
         compiler_params=pltpu.CompilerParams(
-            collective_id=0, has_side_effects=True, vmem_limit_bytes=64 * 2**20 - 420 * 2**10
+            collective_id=0, has_side_effects=True, vmem_limit_bytes=64 * 2**20 - 900 * 2**10
         ),
     )(
         context,

time: 49.8 us -> 44 us (0.88)
  Pallas kernels: 46.9 us -> 42 us
  other arithmetic: 2.12 us -> 1.22 us
    pallas_call x1, Pallas kernels: 46.9 us -> 42 us  [body(): pl.pallas_call(functools.partial(kernel, n_sp, n_tp, block), name='delta'...]
    unnamed x1, other arithmetic: 1.54 us -> 0.64 us
where the time goes in v3:
time: 44 us; the launch traced here: 43.9 us
  Pallas kernels  42 us (95%)
  other arithmetic  1.22 us (3%)
  between operations  0.64 us (1%)
    pallas_call x1, Pallas kernels, body(): pl.pallas_call(functools.partial(kernel, n_sp, n_tp, block), name='delta'...  42 us

profile of v3, /device:TPU:0, one launch (start us, length us, event | category | flops | bytes accessed | tf_op | source)
XLA Modules:
  0.0 43.9 jit_solution(8280473335478946254)
XLA Ops:
  0.6 42.0 %delta.1 = (f32[2,128,128]{2,1,0:T(8,128)S(1)}, f32[2,512]{1,0:T(2,128)S(1)}) custom-call(bf16[2,256,512]{2,1,0:T(8,128)(2,1)} %ctx.1, bf16[2,4096]{1,0:T(2,128)(2,1)} %first_hbm.1, bf16[4096,128]{1,0:T(8,128)(2,1)} %wk_hbm.1, bf16[4096,128]{1,0:T(8,128)(2,1)} %wv_hbm.1, bf16[4096,128]{1,0:T(8,128)(2,1)} %wq_hbm.1, bf16[4096,128]{1,0:T(8,128)(2,1)} %wz_hbm.1, ...), custom_call_target="tpu_custom_call" | custom-call | tf_op jit(solution)/shard_map/delta/pallas_call | solution.py:554
  42.7 0.6 %convert_bitcast_fusion = bf16[2,1,1,128,128]{4,3,2,1,0:T(8,128)(2,1)} fusion(f32[2,128,128]{2,1,0:T(8,128)S(1)} %get-tuple-element.4), kind=kLoop, calls=%fused_computation | loop fusion | flops 32768 | bytes 196608
  43.3 0.6 %convert_element_type.11 = bf16[2,512]{1,0:T(2,128)(2,1)} convert(f32[2,512]{1,0:T(2,128)S(1)} %get-tuple-element.5) | non-fusion elementwise | flops 1024 | bytes 6144 | tf_op jit(solution)/shard_map/convert_element_type | solution.py:615
